TPU v7x, 768 devices: a whole 4x8x12 slice. The times are simulated.
768 devices in a mesh: row: 48 (over z, x), col: 16 (over y, core).
Axes of the slice: x: 4, y: 8, z: 12, core: 2. Of those that a mesh axis runs over, the one named last changes fastest.
Arguments:
- tokens: bfloat16 [55296, 4096], P('row'), may hold values from -6 to 6
- proj_in: bfloat16 [4096, 2048], P(None, 'col'), may hold values from -0.09375 to 0.09375
- proj_out: bfloat16 [2048, 4096], P(None, 'col'), may hold values from -0.125 to 0.125
Outputs:
- mixed: bfloat16 [55296, 4096], P('row', 'col')
All inputs are finite; a program needn't handle non-finite values.
Results may differ from a plain program's by a relative error of at most 0.0057.
Values may be sent and summed in bfloat16 or wider, within the bound.
A program may use at most 64 MiB of HBM per device.

v0:
```python
import math

import jax
import jax.numpy as jnp
from jax import lax
from jax.sharding import PartitionSpec as P


def cos_sin(row_ids, col_ids, period):
    phase_idx = row_ids * col_ids % period
    angles = phase_idx.astype(jnp.float32) * (2.0 * math.pi / period)
    return (jnp.cos(angles), jnp.sin(angles))


def apply_table(form, table_cos, table_sin, real_part, imag_part):
    highest = lax.Precision.HIGHEST
    out_real = jnp.einsum(form, table_cos, real_part, precision=highest) + jnp.einsum(
        form, table_sin, imag_part, precision=highest
    )
    out_imag = jnp.einsum(form, table_cos, imag_part, precision=highest) - jnp.einsum(
        form, table_sin, real_part, precision=highest
    )
    return (out_real, out_imag)


def on_device(tokens, proj_in, proj_out):
    row_count = lax.axis_size("row")
    local_rows = tokens.shape[0]
    group_width = proj_in.shape[1]
    seq_length = local_rows * row_count
    row_rank = lax.axis_index("row")
    highest = lax.Precision.HIGHEST
    first_len = 16
    second_len = local_rows // first_len
    branch_in = jnp.dot(tokens, proj_in, preferred_element_type=jnp.float32).astype(jnp.bfloat16)
    outer_idx = jnp.arange(row_count, dtype=jnp.int32)
    outer_cos, outer_sin = cos_sin(outer_idx[:, None], outer_idx[None, :], row_count)
    values = lax.all_to_all(
        branch_in.reshape(1, local_rows, group_width),
        "row",
        split_axis=1,
        concat_axis=0,
        tiled=True,
    ).astype(jnp.float32)
    real_part = jnp.einsum("kn,nmg->kmg", outer_cos, values, precision=highest)
    imag_part = -jnp.einsum("kn,nmg->kmg", outer_sin, values, precision=highest)
    real_parts = real_part
    imag_parts = imag_part
    inner_idx = jnp.arange(local_rows, dtype=jnp.int32)
    first_idx = jnp.arange(first_len, dtype=jnp.int32)
    second_idx = jnp.arange(second_len, dtype=jnp.int32)
    first_cos, first_sin = cos_sin(first_idx[:, None], first_idx[None, :], first_len)
    second_cos, second_sin = cos_sin(second_idx[:, None], second_idx[None, :], second_len)
    mid_cos, mid_sin = cos_sin(first_idx[:, None], second_idx[None, :], local_rows)
    mid_cos = mid_cos[None, :, :, None]
    mid_sin = mid_sin[None, :, :, None]
    twid_cos, twid_sin = cos_sin(row_rank, inner_idx, seq_length)
    twid_cos = twid_cos[None, :, None]
    twid_sin = twid_sin[None, :, None]
    real_part = lax.all_to_all(real_parts, "row", split_axis=0, concat_axis=1, tiled=True)
    imag_part = lax.all_to_all(imag_parts, "row", split_axis=0, concat_axis=1, tiled=True)
    real_part, imag_part = (
        real_part * twid_cos + imag_part * twid_sin,
        imag_part * twid_cos - real_part * twid_sin,
    )
    leading = real_part.shape[0]
    items = real_part.shape[2]
    real_part = real_part.reshape(leading, first_len, second_len, items)
    imag_part = imag_part.reshape(leading, first_len, second_len, items)
    real_part, imag_part = apply_table("kn,anqg->akqg", first_cos, first_sin, real_part, imag_part)
    real_part, imag_part = (
        real_part * mid_cos + imag_part * mid_sin,
        imag_part * mid_cos - real_part * mid_sin,
    )
    real_part, imag_part = apply_table(
        "kq,apqg->akpg", second_cos, second_sin, real_part, imag_part
    )
    spec_real = real_part.reshape(leading, local_rows, items)
    spec_imag = imag_part.reshape(leading, local_rows, items)
    channel = jnp.arange(group_width, dtype=jnp.int32)
    chan_cos, chan_sin = cos_sin(channel[:, None], channel[None, :], group_width)
    norm_scale = 1.0 / math.sqrt(seq_length * group_width)
    mixed_real = (
        jnp.dot(
            spec_real.reshape(local_rows, group_width),
            chan_cos,
            precision=highest,
            preferred_element_type=jnp.float32,
        )
        + jnp.dot(
            spec_imag.reshape(local_rows, group_width),
            chan_sin,
            precision=highest,
            preferred_element_type=jnp.float32,
        )
    ) * norm_scale
    spectrum = mixed_real.astype(jnp.bfloat16)
    returned = lax.all_to_all(
        spectrum.reshape(local_rows, 1, group_width), "row", split_axis=0, concat_axis=1, tiled=True
    )
    returned = returned.reshape(local_rows, group_width)
    output_sum = jnp.dot(
        lax.all_gather(returned, "col", axis=1, tiled=True),
        proj_out,
        preferred_element_type=jnp.float32,
    )
    return output_sum.astype(jnp.bfloat16)


def solution(mesh):
    return jax.shard_map(
        on_device,
        mesh=mesh,
        in_specs=(P("row", None), P(None, "col"), P(None, "col")),
        out_specs=P("row", "col"),
        check_vma=False,
    )
```

profile of v0, /device:TPU:1, one launch (start us, length us, event | category | flops | bytes accessed | tf_op | source)
XLA Modules:
  0.0 225.3 jit_solution(8309479698489988533)
XLA Ops:
  6.5 6.6 %fusion.2 = bf16[1,1152,128]{2,1,0:T(8,128)(2,1)S(1)} fusion(bf16[1152,4096]{1,0:T(8,128)(2,1)} %param.3, bf16[4096,128]{1,0:T(8,128)(2,1)} %param.4), kind=kOutput, calls=%fused_computation.5 | convolution fusion | flops 1208107008 | bytes 10780672 | tf_op jit(solution)/shard_map/dot_general | solution.py:35
  13.1 4.6 %copy.106 = bf16[1,1152,128]{2,0,1:T(2,128)(2,1)S(1)} copy(bf16[1,1152,128]{2,1,0:T(8,128)(2,1)S(1)} %fusion.2) | data formatting | bytes 589824 | tf_op jit(solution)/shard_map/reshape | solution.py:39
  17.8 0.5 broadcast.161
  18.3 6.7 %reduce = bf16[1152,128]{1,0:T(8,128)(2,1)S(1)} reduce(bf16[1152,1,128]{2,1,0:T(2,128)(2,1)S(1)} %bitcast.89, bf16[]{:T(256)} %broadcast.161), dimensions={1}, to_apply=%bitcast.84.reduce_sub_computation | reduce | bytes 589826
  25.1 36.2 %all_to_all.51 = bf16[48,2,1536]{2,1,0:T(2,128)(2,1)S(1)} all-to-all(bf16[48,2,1536]{2,1,0:T(2,128)(2,1)S(1)} %reshape.175), channel_id=1, replica_groups=mesh['row'=48,'col'=16] {'row'}, dimensions={0} | all-to-all | bytes 589824 | tf_op jit(solution)/shard_map/all_to_all | solution.py:38
  61.4 0.2 reshape.176
  61.7 0.5 convolution_negate_fusion
  62.2 1.0 copy.66
  63.2 5.5 %all-to-all-start.2 = ((f32[48,24,128]{2,1,0:T(8,128)}), f32[48,24,128]{2,1,0:T(8,128)S(1)}, u32[]{:S(2)}, u32[]{:S(2)}) async-start(f32[48,24,128]{2,1,0:T(8,128)} %copy.66), calls=%async_computation.2 | async-start | bytes 1179648 | tf_op jit(solution)/shard_map/all_to_all | solution.py:61
  68.7 0.5 fusion.23
  69.2 1.0 copy.64
  70.2 24.2 %all-to-all-done.2 = f32[48,24,128]{2,1,0:T(8,128)S(1)} async-done(((f32[48,24,128]{2,1,0:T(8,128)}), f32[48,24,128]{2,1,0:T(8,128)S(1)}, u32[]{:S(2)}, u32[]{:S(2)}) %all-to-all-start.2) | async-done | bytes 589856 | tf_op jit(solution)/shard_map/all_to_all | solution.py:61
  94.4 6.4 %all-to-all-start.1 = ((f32[48,24,128]{2,1,0:T(8,128)}), f32[48,24,128]{2,1,0:T(8,128)S(1)}, u32[]{:S(2)}, u32[]{:S(2)}) async-start(f32[48,24,128]{2,1,0:T(8,128)} %copy.64), calls=%async_computation.1 | async-start | bytes 1179648 | tf_op jit(solution)/shard_map/all_to_all | solution.py:60
  100.7 0.2 all-gather.2.cloned.1.call-start
  101.4 25.2 %all-to-all-done.1 = f32[48,24,128]{2,1,0:T(8,128)S(1)} async-done(((f32[48,24,128]{2,1,0:T(8,128)}), f32[48,24,128]{2,1,0:T(8,128)S(1)}, u32[]{:S(2)}, u32[]{:S(2)}) %all-to-all-start.1) | async-done | bytes 589856 | tf_op jit(solution)/shard_map/all_to_all | solution.py:60
  126.6 0.4 fusion.8
  127.0 0.7 fusion.20
  127.7 0.7 fusion.16
  128.4 0.7 fusion.6
  129.1 0.9 subtract_bitcast_fusion
  130.0 0.9 fusion.10
  130.9 0.9 fusion.14
  131.8 0.9 fusion.4
  132.7 0.9 fusion.5
  133.8 0.9 fusion.29
  134.8 0.9 fusion.3
  135.7 0.8 reduce.1
  136.6 20.9 %all_to_all.52 = bf16[48,2,1536]{2,1,0:T(2,128)(2,1)S(1)} all-to-all(bf16[48,2,1536]{2,1,0:T(2,128)(2,1)S(1)} %reshape.177), channel_id=1, replica_groups=mesh['row'=48,'col'=16] {'row'}, dimensions={0} | all-to-all | bytes 589824 | tf_op jit(solution)/shard_map/all_to_all | solution.py:98
  157.5 0.2 reshape.178
  157.8 0.8 copy.80
  158.6 55.4 %all-gather.2.cloned.1.call-done = bf16[1152,2048]{1,0:T(8,128)(2,1)} async-done(((bf16[1152,128]{1,0:T(8,128)(2,1)}), bf16[1152,2048]{1,0:T(8,128)(2,1)}) %all-gather.2.cloned.1.call-update) | async-done | bytes 4718608 | tf_op jit(solution)/shard_map/all_gather | solution.py:103
  213.9 4.5 %convolution_convert_fusion = bf16[1152,256]{1,0:T(8,128)(2,1)} fusion(bf16[1152,2048]{1,0:T(8,128)(2,1)} %all-gather.2.cloned.1.call-done, bf16[2048,256]{1,0:T(8,128)(2,1)S(1)} %copy-done), kind=kOutput, calls=%fused_computation | convolution fusion | flops 1208254464 | bytes 6356992 | tf_op jit(solution)/shard_map/dot_general | solution.py:102
  (14 shorter events, 0.9 us)
Async XLA Ops:
  6.5 207.4 %copy-start = (bf16[2048,256]{1,0:T(8,128)(2,1)S(1)}, bf16[2048,256]{1,0:T(8,128)(2,1)}, u32[]{:S(2)}) copy-start(bf16[2048,256]{1,0:T(8,128)(2,1)} %param.5) | copy-start | bytes 3145732
  63.2 31.2 %all-to-all-start.2 = ((f32[48,24,128]{2,1,0:T(8,128)}), f32[48,24,128]{2,1,0:T(8,128)S(1)}, u32[]{:S(2)}, u32[]{:S(2)}) async-start(f32[48,24,128]{2,1,0:T(8,128)} %copy.66), calls=%async_computation.2 | async-start | bytes 1179648 | tf_op jit(solution)/shard_map/all_to_all | solution.py:61
  94.4 32.2 %all-to-all-start.1 = ((f32[48,24,128]{2,1,0:T(8,128)}), f32[48,24,128]{2,1,0:T(8,128)S(1)}, u32[]{:S(2)}, u32[]{:S(2)}) async-start(f32[48,24,128]{2,1,0:T(8,128)} %copy.64), calls=%async_computation.1 | async-start | bytes 1179648 | tf_op jit(solution)/shard_map/all_to_all | solution.py:60
  100.7 113.2 %all-gather.2.cloned.1.call-start = ((), (), s32[]{:S(2)}) async-start(), calls=%async_computation.4 | async-start | bytes 5013504 | tf_op jit(solution)/shard_map/all_gather | solution.py:103
Sparse Core Ops, SparseCore 0:
  158.7 55.2 all-gather.1
where the time goes:
time: 226 us; the launch traced here: 225 us
  waiting for transfers between devices  105 us (46%)
  blocking collectives  57.1 us (25%)
  matrix products  20.5 us (9%)
  between operations  13.6 us (6%)
  starting transfers between devices  12.1 us (5%)
  local copies, waits for them, and re-layouts  9.05 us (4%)
  other arithmetic  8.14 us (4%)
    all_gather x1, waiting for transfers between devices, on_device(): lax.all_gather(returned, 'col', axis=1, tiled=True)  55.4 us
    all_to_all x1, blocking collectives, on_device(): lax.all_to_all(branch_in.reshape(1, local_rows, group_width), 'row', spli...  36.2 us
    all_to_all x1, waiting for transfers between devices, on_device(): lax.all_to_all(real_parts, 'row', split_axis=0, concat_axis=1, tiled=True)  25.2 us
    all_to_all x1, waiting for transfers between devices, on_device(): lax.all_to_all(imag_parts, 'row', split_axis=0, concat_axis=1, tiled=True)  24.2 us
    all_to_all x1, blocking collectives, on_device(): lax.all_to_all(spectrum.reshape(local_rows, 1, group_width), 'row', split...  20.9 us
    unnamed x1, other arithmetic  6.75 us
    dot_general x1, matrix products, on_device(): jnp.dot(tokens, proj_in, preferred_element_type=jnp.float32)  6.61 us
    all_to_all x1, starting transfers between devices, on_device(): lax.all_to_all(real_parts, 'row', split_axis=0, concat_axis=1, tiled=True)  6.36 us
  transfers between devices with their start and end apart: 3, of which 3 were waited for; matrix products, arithmetic and copies ran while one was open for 1% of the time, Pallas kernels for 0%

commit v1 on v0

v1 whole, which is shorter than its diff:
```python
import functools
import math

import jax
import jax.numpy as jnp
import numpy as np
from jax import lax
from jax.experimental import pallas as pl
from jax.experimental.pallas import tpu as pltpu
from jax.sharding import PartitionSpec as P

MESH = pl.DeviceIdType.MESH
BF16 = jnp.bfloat16
F32 = jnp.float32


def exchange_kernel(n, src, dst, send_sem, recv_sem):
    me = lax.axis_index("row")
    barrier = pltpu.get_barrier_semaphore()

    def greet(s, carry):
        peer = lax.rem(me + s, n)
        pl.semaphore_signal(barrier, inc=1, device_id={"row": peer}, device_id_type=MESH)
        return carry

    lax.fori_loop(1, n, greet, 0)
    pl.semaphore_wait(barrier, n - 1)

    def send(s, carry):
        peer = lax.rem(me + s, n)
        pltpu.make_async_remote_copy(
            src_ref=src.at[peer],
            dst_ref=dst.at[me],
            send_sem=send_sem,
            recv_sem=recv_sem,
            device_id={"row": peer},
            device_id_type=MESH,
        ).start()
        return carry

    lax.fori_loop(1, n, send, 0)
    dst[me] = src[me]
    rest = dst.at[pl.ds(0, n - 1)]
    pltpu.make_async_copy(rest, rest, recv_sem).wait()
    pltpu.make_async_copy(rest, rest, send_sem).wait()


def exchange(blocks, ident):
    n = blocks.shape[0]
    return pl.pallas_call(
        functools.partial(exchange_kernel, n),
        out_shape=jax.ShapeDtypeStruct(blocks.shape, blocks.dtype),
        in_specs=[pl.BlockSpec(memory_space=pltpu.VMEM)],
        out_specs=pl.BlockSpec(memory_space=pltpu.VMEM),
        scratch_shapes=[pltpu.SemaphoreType.DMA, pltpu.SemaphoreType.DMA],
        compiler_params=pltpu.CompilerParams(collective_id=ident, has_side_effects=True),
    )(blocks)


def cos_sin(phase, period):
    angles = phase.astype(F32) * (2.0 * math.pi / period)
    return jnp.cos(angles), jnp.sin(angles)


def channel_table(width):
    half = width // 2
    j = np.arange(width)
    l = np.arange(half)
    table = np.zeros((width, width))
    table[:, :half] = np.cos(2 * np.pi * np.outer(j, l) / width)
    table[:, half:] = -np.sin(2 * np.pi * np.outer(j, l) / width)
    table[:, half] = (-1.0) ** j
    return table


def on_device(tokens, proj_in, proj_out):
    n = lax.axis_size("row")
    rank = lax.axis_index("row")
    rows = tokens.shape[0]
    width = proj_in.shape[1]
    half = width // 2
    total = rows * n
    inner = rows // n
    branch_in = jnp.dot(tokens, proj_in, preferred_element_type=F32).astype(BF16)
    chan = jnp.asarray(channel_table(width), BF16)
    mixed = jnp.dot(branch_in, chan, preferred_element_type=F32).astype(BF16)
    blocks = mixed.reshape(inner, n, width).transpose(1, 0, 2)
    data = exchange(blocks, 0).reshape(rows, width)
    d = np.arange(n)[:, None]
    a = np.arange(inner)[None, :]
    freq = np.where(a < inner // 2, 48 * a + d, n * a + (n - d) % n).reshape(-1)
    times = n * jnp.arange(rows, dtype=jnp.int32) + rank
    phase = (jnp.asarray(freq, jnp.int32)[:, None] * times[None, :]) % total
    tc, ts = cos_sin(phase, total)
    g = jnp.dot(tc.astype(BF16), data, preferred_element_type=F32)
    h = jnp.dot(ts.astype(BF16), data, preferred_element_type=F32)
    g = g + jnp.concatenate([h[:, half:], -h[:, :half]], axis=1)
    parts = exchange(g.astype(BF16).reshape(n, inner, width), 1)
    mirror = jnp.where(rank == 0, (inner - np.arange(inner)) % inner, inner - 1 - np.arange(inner))
    other = jnp.take(parts, mirror, axis=1)
    b = np.arange(n)
    p = np.arange(n)

    def tab(rows_):
        ang = 2 * np.pi * (np.outer(rows_, p) % n) / n
        return np.concatenate([np.cos(ang), np.sin(ang)], axis=1)

    fwd = jnp.asarray(tab(b), BF16)
    rev = jnp.asarray(tab(n - 1 - b), BF16)
    rev0 = jnp.asarray(tab((n - b) % n), BF16)
    er, ei = parts[:, :, :half], parts[:, :, half:]
    fr, fi = other[:, :, :half], other[:, :, half:]
    first = (np.arange(half) == 0)[None, None, :]
    zero = jnp.zeros_like(er)
    half_ = jnp.asarray(0.5, BF16)
    x1 = jnp.concatenate([jnp.where(first, er * half_, er), jnp.where(first, ei * half_, zero)], axis=2)
    x2 = jnp.concatenate([jnp.where(first, ei * half_, ei), jnp.where(first, -er * half_, zero)], axis=2)
    x3 = jnp.concatenate([jnp.where(first, fr * half_, zero), jnp.where(first, fi * half_, fr)], axis=2)
    x4 = jnp.concatenate([jnp.where(first, fi * half_, zero), jnp.where(first, -fr * half_, fi)], axis=2)
    xa = jnp.concatenate([x1, x2], axis=0)
    xb = jnp.concatenate([x3, x4], axis=0)
    out = jnp.einsum("bp,pal->bal", fwd, xa, preferred_element_type=F32)
    out_m = jnp.einsum("bp,pal->bal", rev, xb, preferred_element_type=F32)
    out_0 = jnp.einsum("bp,pl->bl", rev0, xb[:, 0], preferred_element_type=F32)
    out_m = jnp.concatenate([jnp.where(rank == 0, out_0, out_m[:, 0])[:, None], out_m[:, 1:]], axis=1)
    spec = ((out + out_m) * (1.0 / math.sqrt(total * width))).astype(BF16)
    last = exchange(spec, 2)
    low = last[:, : inner // 2].transpose(1, 0, 2)
    up = last[:, inner // 2 :]
    up = jnp.concatenate([up[:1], up[1:][::-1]], axis=0).transpose(1, 0, 2)
    spectrum = jnp.concatenate([low, up], axis=0).reshape(rows, width)
    perm = np.concatenate([np.arange(half), [half], width - np.arange(1, half)])
    weights = proj_out.reshape(-1, width, proj_out.shape[1])[:, perm].reshape(proj_out.shape)
    gathered = lax.all_gather(spectrum, "col", axis=1, tiled=True)
    return jnp.dot(gathered, weights, preferred_element_type=F32).astype(BF16)


def solution(mesh):
    return jax.shard_map(
        on_device,
        mesh=mesh,
        in_specs=(P("row", None), P(None, "col"), P(None, "col")),
        out_specs=P("row", "col"),
        check_vma=False,
    )
```

time: 226 us -> 217 us (0.960)
  Pallas kernels: 0 us -> 72.9 us
  blocking collectives: 57.1 us -> 0 us
  waiting for transfers between devices: 105 us -> 57.3 us
  matrix products: 20.5 us -> 60.2 us
  starting transfers between devices: 12.1 us -> 0.01 us
  other arithmetic: 8.14 us -> 4.23 us
    pallas_call x0 -> x3, Pallas kernels: none -> 72.9 us  [exchange(): pl.pallas_call(functools.partial(exchange_kernel, n), out_shape=jax.Shape...]
    all_to_all x2 -> x0, blocking collectives: 57.1 us -> none  [the longest x1 36.2 us: on_device(): lax.all_to_all(branch_in.reshape(1, local_rows, group_width), 'row', spli...]
    all_to_all x2 -> x0, waiting for transfers between devices: 49.4 us -> none  [the longest x1 25.2 us: on_device(): lax.all_to_all(real_parts, 'row', split_axis=0, concat_axis=1, tiled=True)]
    dot_general x14 -> x7, matrix products: 20.5 us -> 60.2 us  [the longest x1 25.8 us: on_device(): h = jnp.dot(ts.astype(BF16), data, preferred_element_type=F32)]
    all_to_all x2 -> x0, starting transfers between devices: 11.9 us -> none  [the longest x1 6.36 us: on_device(): lax.all_to_all(real_parts, 'row', split_axis=0, concat_axis=1, tiled=True)]
    unnamed x1 -> x0, other arithmetic: 6.75 us -> none
    reshape x1 -> x2, local copies, waits for them, and re-layouts: 4.6 us -> 1.38 us  [the longest x1 0.8 us: on_device(): blocks = mixed.reshape(inner, n, width).transpose(1, 0, 2)]
  transfers between devices with their start and end apart: 3 -> 1, of which waited for: 3 -> 1; matrix products, arithmetic and copies ran while one was open for 1% -> 1% of each run, Pallas kernels for 0% -> 0%
where the time goes in v1:
time: 217 us; the launch traced here: 216 us
  Pallas kernels  72.9 us (34%)
  matrix products  60.2 us (28%)
  waiting for transfers between devices  57.3 us (26%)
  between operations  13.7 us (6%)
  local copies, waits for them, and re-layouts  8.11 us (4%)
  other arithmetic  4.23 us (2%)
    pallas_call x3, Pallas kernels, exchange(): pl.pallas_call(functools.partial(exchange_kernel, n), out_shape=jax.Shape...  72.9 us
    all_gather x1, waiting for transfers between devices, on_device(): gathered = lax.all_gather(spectrum, 'col', axis=1, tiled=True)  57.3 us
    dot_general x1, matrix products, on_device(): h = jnp.dot(ts.astype(BF16), data, preferred_element_type=F32)  25.8 us
    dot_general x1, matrix products, on_device(): g = jnp.dot(tc.astype(BF16), data, preferred_element_type=F32)  22.9 us
    dot_general x1, matrix products, on_device(): mixed = jnp.dot(branch_in, chan, preferred_element_type=F32).astype(BF16)  6.49 us
    dot_general x1, matrix products, on_device(): return jnp.dot(gathered, weights, preferred_element_type=F32).astype(BF16)  4.54 us
  transfers between devices with their start and end apart: 1, of which 1 were waited for; matrix products, arithmetic and copies ran while one was open for 1% of the time, Pallas kernels for 0%

profile of v1, /device:TPU:1, one launch (start us, length us, event | category | flops | bytes accessed | tf_op | source)
XLA Modules:
  0.0 216.5 jit_solution(17562806117918290379)
XLA Ops:
  6.6 0.8 compare_and_fusion
  7.3 0.5 copy-done
  7.8 6.5 %convolution_convert_fusion.1 = bf16[1152,128]{1,0:T(8,128)(2,1)S(1)} fusion(bf16[128,128]{1,0:T(8,128)(2,1)} %constant.65.clone, bf16[1152,4096]{1,0:T(8,128)(2,1)} %param.13, bf16[4096,128]{1,0:T(8,128)(2,1)S(1)} %copy-done), kind=kOutput, calls=%fused_computation.16 | convolution fusion | flops 1246003200 | bytes 10813440 | tf_op jit(solution)/shard_map/dot_general | solution.py:86
  14.3 0.8 copy.58
  15.1 29.6 %shard_map.127 = bf16[48,24,128]{2,1,0:T(8,128)(2,1)} custom-call(bf16[48,24,128]{2,1,0:T(8,128)(2,1)} %bitcast.38), custom_call_target="tpu_custom_call" | custom-call | tf_op jit(solution)/shard_map/pallas_call | solution.py:50
  44.7 25.8 %fusion.6 = f32[1152,128]{1,0:T(8,128)S(1)} fusion(bf16[1152,128]{1,0:T(8,128)(2,1)} %bitcast.41, s32[1152]{0:T(1024)S(1)} %multiply_add_fusion, s32[1152]{0:T(1024)S(1)} %copy-done.8), kind=kOutput, calls=%fused_computation.12 | convolution fusion | flops 353009664 | bytes 893952 | tf_op jit(solution)/shard_map/dot_general | solution.py:96
  70.5 0.2 fusion.24
  70.8 0.0 copy-start.7
  70.8 22.9 %fusion.8 = bf16[1152,128]{1,0:T(8,128)(2,1)} fusion(bf16[1152,128]{1,0:T(8,128)(2,1)S(1)} %bitcast.42, s32[1152]{0:T(1024)S(1)} %multiply_add_fusion, s32[1152]{0:T(1024)S(1)} %copy-done.8, f32[1152,64]{1,0:T(8,128)S(1)} %get-tuple-element.8, f32[1152,64]{1,0:T(8,128)S(1)} %get-tuple-element.7), kind=kOutput, calls=%fused_computation.15 | convolution fusion | flops 353452032 | bytes 1188864 | tf_op jit(solution)/shard_map/dot_general | solution.py:95
  93.6 21.1 %shard_map.128 = bf16[48,24,128]{2,1,0:T(8,128)(2,1)} custom-call(bf16[48,24,128]{2,1,0:T(8,128)(2,1)} %bitcast.43), custom_call_target="tpu_custom_call" | custom-call | tf_op jit(solution)/shard_map/pallas_call | solution.py:50
  114.8 1.0 copy.34
  115.8 0.6 gather_fusion
  116.4 0.1 fusion.15
  116.5 1.4 multiply_select_fusion
  117.9 0.7 maximum_maximum_fusion
  118.6 0.2 fusion.11
  118.9 0.2 copy.44
  119.1 0.2 fusion.13
  119.3 0.1 convolution_select_fusion
  119.5 1.0 fusion.10.src
  120.5 22.2 %shard_map.129 = bf16[48,24,128]{2,1,0:T(8,128)(2,1)} custom-call(bf16[48,24,128]{2,1,0:T(8,128)(2,1)} %fusion.10.src), custom_call_target="tpu_custom_call" | custom-call | tf_op jit(solution)/shard_map/pallas_call | solution.py:50
  142.6 0.7 slice.49
  143.3 1.0 slice.50
  144.3 0.9 slice_bitcast_fusion
  145.3 0.1 pad_maximum_fusion
  145.4 0.8 copy.39
  146.2 0.0 all-gather.2.cloned.1.call-update
  146.2 0.6 copy.40
  146.8 0.6 gather_fusion.1
  147.5 0.3 copy.41
  147.8 57.3 %all-gather.2.cloned.1.call-done = bf16[1152,2048]{1,0:T(8,128)(2,1)} async-done(((bf16[1152,128]{1,0:T(8,128)(2,1)}), bf16[1152,2048]{1,0:T(8,128)(2,1)}) %all-gather.2.cloned.1.call-update) | async-done | bytes 4718608 | tf_op jit(solution)/shard_map/all_gather | solution.py:134
  205.1 4.5 %convolution_convert_fusion = bf16[1152,256]{1,0:T(8,128)(2,1)} fusion(bf16[1152,2048]{1,0:T(8,128)(2,1)} %all-gather.2.cloned.1.call-done, bf16[2048,256]{1,0:T(8,128)(2,1)S(1)} %bitcast.40), kind=kOutput, calls=%fused_computation.13 | convolution fusion | flops 1208254464 | bytes 6356992 | tf_op jit(solution)/shard_map/dot_general | solution.py:135
  (24 shorter events, 0.2 us)
Async XLA Ops:
  6.5 1.2 copy-start
  6.5 198.6 %all-gather.2.cloned.1.call-start = ((), (), s32[]{:S(2)}) async-start(), calls=%async_computation | async-start | bytes 5013504 | tf_op jit(solution)/shard_map/all_gather | solution.py:134
  7.8 36.9 %copy-start.8 = (s32[1152]{0:T(1024)S(1)}, s32[1152]{0:T(1024)}, u32[]{:S(2)}) copy-start(s32[1152]{0:T(1024)} %constant.66.clone) | copy-start | bytes 13828
  44.7 26.0 %copy-start.2 = (bf16[48,24,128]{2,1,0:T(8,128)(2,1)S(1)}, bf16[48,24,128]{2,1,0:T(8,128)(2,1)}, u32[]{:S(2)}) copy-start(bf16[48,24,128]{2,1,0:T(8,128)(2,1)} %shard_map.127) | copy-start | bytes 884740
  70.8 45.7 %copy-start.7 = (pred[64]{0:T(512)(128)(4,1)S(1)}, pred[64]{0:T(512)(128)(4,1)}, u32[]{:S(2)}) copy-start(pred[64]{0:T(512)(128)(4,1)} %constant.75) | copy-start | bytes 196
  93.6 25.0 %copy-start.4 = (bf16[48,96,1]{1,0,2:T(8,128)(2,1)S(1)}, bf16[48,96,1]{1,0,2:T(8,128)(2,1)}, u32[]{:S(2)}) copy-start(bf16[48,96,1]{1,0,2:T(8,128)(2,1)} %constant.79) | copy-start | bytes 27652
  116.5 2.6 %copy-start.3 = (bf16[48,96,1]{1,0,2:T(8,128)(2,1)S(1)}, bf16[48,96,1]{1,0,2:T(8,128)(2,1)}, u32[]{:S(2)}) copy-start(bf16[48,96,1]{1,0,2:T(8,128)(2,1)} %constant.78) | copy-start | bytes 27652
  116.5 2.8 %copy-start.5 = (bf16[48,96]{1,0:T(8,128)(2,1)S(1)}, bf16[48,96]{1,0:T(8,128)(2,1)}, u32[]{:S(2)}) copy-start(bf16[48,96]{1,0:T(8,128)(2,1)} %constant.71.clone) | copy-start | bytes 27652
  118.5 27.7 %copy-start.1 = (bf16[2048,256]{1,0:T(8,128)(2,1)S(1)}, bf16[2048,256]{1,0:T(8,128)(2,1)}, u32[]{:S(2)}) copy-start(bf16[2048,256]{1,0:T(8,128)(2,1)} %param.15) | copy-start | bytes 3145732
  118.8 28.0 %copy-start.6 = (s32[128]{0:T(128)S(1)}, s32[128]{0:T(128)}, u32[]{:S(2)}) copy-start(s32[128]{0:T(128)} %constant.77) | copy-start | bytes 1540
Sparse Core Ops, SparseCore 0:
  146.3 58.7 all-gather.1

commit v2 on v1

v2 whole, which is shorter than its diff:
```python
import functools
import math

import jax
import jax.numpy as jnp
from jax import lax
from jax.experimental import pallas as pl
from jax.experimental.pallas import tpu as pltpu
from jax.sharding import PartitionSpec as P

MESH = pl.DeviceIdType.MESH
BF16 = jnp.bfloat16
F32 = jnp.float32
CHUNKS = 3


def turn(phase, period):
    wraps = jnp.floor(phase * (1.0 / period) + 0.5)
    x = (phase - wraps * period) * (math.pi / period)
    y = x * x
    s = 1.0 + y * (-1 / 6 + y * (1 / 120 + y * (-1 / 5040 + y * (1 / 362880 + y * (-1 / 39916800)))))
    c = 1.0 + y * (
        -1 / 2 + y * (1 / 24 + y * (-1 / 720 + y * (1 / 40320 + y * (-1 / 3628800 + y * (1 / 479001600)))))
    )
    s = s * x
    return 1.0 - 2.0 * s * s, 2.0 * s * c


def iota(shape, axis):
    return lax.broadcasted_iota(jnp.int32, shape, axis)


def dot(a, b):
    return jnp.dot(a, b, preferred_element_type=F32)


def kernel(
    n,
    ncol,
    tokens,
    proj_in,
    proj_out,
    out,
    tok,
    win,
    wout,
    table,
    base_c,
    base_s,
    work,
    gacc,
    send1,
    recv1,
    send2,
    recv2,
    send3,
    recv3,
    gath,
    upper,
    load_sem,
    xs,
    xr,
    rs_sem,
    rr_sem,
    ls_sem,
    lr_sem,
    ss_sem,
    sr_sem,
):
    rank = lax.axis_index("row")
    col = lax.axis_index("col")
    core = lax.rem(col, 2)
    right = lax.rem(col + 2, ncol)
    left = lax.rem(col + ncol - 2, ncol)
    sib = col + 1 - 2 * core
    rows, depth = tokens.shape
    width = proj_in.shape[1]
    half = width // 2
    total = rows * n
    part = rows // CHUNKS
    per = part // n

    barrier = pltpu.get_barrier_semaphore()

    def greet(s, carry):
        pl.semaphore_signal(
            barrier, inc=1, device_id={"row": lax.rem(rank + s, n)}, device_id_type=MESH
        )
        return carry

    lax.fori_loop(1, n, greet, 0)
    for peer in (right, left, sib):
        pl.semaphore_signal(barrier, inc=1, device_id={"col": peer}, device_id_type=MESH)

    load_in = pltpu.make_async_copy(proj_in, win, load_sem.at[CHUNKS])
    load_in.start()
    loads = []
    for c in range(CHUNKS):
        block = pl.ds(c * part, part)
        load = pltpu.make_async_copy(tokens.at[block], tok.at[block], load_sem.at[c])
        load.start()
        loads.append(load)
    load_out = pltpu.make_async_copy(proj_out, wout, load_sem.at[CHUNKS + 1])
    load_out.start()

    def post(src, dst, which):
        def send(s, carry):
            peer = lax.rem(rank + s, n)
            pltpu.make_async_remote_copy(
                src_ref=src.at[peer],
                dst_ref=dst.at[rank],
                send_sem=xs.at[which],
                recv_sem=xr.at[which],
                device_id={"row": peer},
                device_id_type=MESH,
            ).start()
            return carry

        lax.fori_loop(1, n, send, 0)
        dst[rank] = src[rank]

    def arrived(dst, which):
        rest = dst.at[pl.ds(0, n - 1)]
        pltpu.make_async_copy(rest, rest, xr.at[which]).wait()

    def flat(ref):
        return ref[...].astype(F32).reshape(part, width)

    def blocks(value):
        return value.reshape(n, per, width).astype(BF16)

    lane = iota((width, width), 1)
    j = iota((width, width), 0)
    l = jnp.where(lane < half, lane, jnp.where(lane == half, half, lane - half))
    cc, sc = turn((j * l).astype(F32), width)
    chan = jnp.where(lane <= half, cc, -sc).astype(BF16)

    load_in.wait()
    for c in range(CHUNKS):
        loads[c].wait()
        x = dot(tok[pl.ds(c * part, part), :], win[...]).astype(BF16)
        work[...] = dot(x, chan)
        for p in range(n):
            send1[c, p] = work[pl.ds(p, per, stride=n), :].astype(BF16)
        if c == 0:
            pl.semaphore_wait(barrier, n - 1 + 3)
        post(send1.at[c], recv1.at[c], c)

    lanes = rows
    li = iota((8, lanes), 1)
    cq = jnp.where(li >= 2 * part, 2, jnp.where(li >= part, 1, 0))
    rem = li - cq * part
    t = n // 2 * (rem // per) + per * cq + rem % per
    time = (n * t + rank).astype(F32)
    ri = iota((8, lanes), 0)
    for g in range(n // 8):
        bc, bs = turn((ri + 8 * g).astype(F32) * time, total)
        base_c[pl.ds(8 * g, 8), :] = bc
        base_s[pl.ds(8 * g, 8), :] = bs
    sigma = jnp.where(ri < 4, 1.0, -1.0).astype(F32)

    def fill(ca, pair, wc, ws, wcs, wss):
        cos, sin = [], []
        for k in range(2):
            bc = base_c[pl.ds(2 * pair + k, 1), :]
            bs = base_s[pl.ds(2 * pair + k, 1), :]
            cos.append(wc * bc - wss * bs)
            sin.append(ws * bc + wcs * bs)
        at = pl.multiple_of(16 * pair, 16)
        table[ca, pl.ds(at, 16), :] = jnp.concatenate(cos, axis=0).astype(BF16)
        table[ca, pl.ds(part + at, 16), :] = jnp.concatenate(sin, axis=0).astype(BF16)

    for ca in range(CHUNKS):
        num = jnp.where(ri < 4, 4 * ca + ri, 17 - 4 * ca + ri)
        wc, ws = turn(num.astype(F32) * time, rows)

        def body(pair, carry, ca=ca, wc=wc, ws=ws):
            fill(ca, pair, wc, ws, wc * sigma, ws * sigma)
            return carry

        lax.fori_loop(0, n // 2, body, 0)
        if ca == 0:
            ac, as_ = turn(jnp.float32(12.0) * time, rows)
            bc1 = base_c[pl.ds(1, 1), :]
            bs1 = base_s[pl.ds(1, 1), :]
            mid = ri == 7
            cos0 = jnp.where(mid, ac, wc)
            sin0 = jnp.where(mid, as_, ws)
            cos1 = wc * bc1 - ws * sigma * bs1
            sin1 = ws * bc1 + wc * sigma * bs1
            table[0, pl.ds(0, 16), :] = jnp.concatenate([cos0, cos1], axis=0).astype(BF16)
            table[0, pl.ds(part, 16), :] = jnp.concatenate([sin0, sin1], axis=0).astype(BF16)

    bi = iota((n, 4 * n), 0)
    pi = iota((n, 4 * n), 1)
    quarter = jnp.where(pi >= 3 * n, 3, jnp.where(pi >= 2 * n, 2, jnp.where(pi >= n, 1, 0)))
    pp = pi - quarter * n

    def outer(flip):
        bb = jnp.where(quarter < 2, bi, flip - bi)
        oc, os = turn((bb * pp).astype(F32), n)
        return jnp.where((quarter == 0) | (quarter == 2), oc, os)

    at_zero = rank == 0
    tab = outer(n - 1)
    tab_zero = jnp.where(at_zero, outer(n), tab).astype(BF16)
    tab = tab.astype(BF16)

    qr = iota((width, width), 0)
    qc = iota((width, width), 1)
    chosen = jnp.where(qr <= half, qr, width + half - qr)
    swap = jnp.where(qc == chosen, 1.0, 0.0).astype(BF16)
    load_out.wait()

    def reorder(g, carry):
        at = pl.ds(pl.multiple_of(g * width, width), width)
        wout[at, :] = dot(swap, wout[at, :]).astype(BF16)
        return carry

    lax.fori_loop(0, ncol, reorder, 0)

    pr = iota((part, part), 0)
    pc = iota((part, part), 1)
    want_i = pr // n
    want_e = pr - want_i * n
    want_d = jnp.where(want_i < 4, want_e, jnp.where(want_e == 0, 0, n - want_e))
    order = jnp.where(pc == want_d * per + want_i, 1.0, 0.0).astype(BF16)

    sign = jnp.where(iota((part, width), 1) < half, 1.0, -1.0).astype(F32)
    for c in range(CHUNKS):
        arrived(recv1.at[c], c)
        data = flat(recv1.at[c]).astype(BF16)
        for ca in range(CHUNKS):
            got = dot(table[ca, :, pl.ds(c * part, part)], data)
            if c > 0:
                got = gacc[ca] + got
            if c < CHUNKS - 1:
                gacc[ca] = got
            else:
                value = got[:part] + pltpu.roll(got[part:], half, 1) * sign
                send2[ca] = blocks(value)
                if ca < 2:
                    post(send2.at[ca], recv2.at[ca], 3 + ca)

    lane48 = iota((n, width), 1)
    m1 = jnp.where((lane48 == 0) | (lane48 == half), 0.5, jnp.where(lane48 < half, 1.0, 0.0)).astype(F32)
    m2 = jnp.where(lane48 == half, -0.5, m1).astype(F32)
    m3 = jnp.where((lane48 == 0) | (lane48 == half), 0.5, 0.0).astype(F32)
    m4 = jnp.where(lane48 > half, 1.0, 0.0).astype(F32)
    m5 = jnp.where(lane48 == half, -0.5, m3).astype(F32)
    scale = 1.0 / math.sqrt(total * width)

    def outer_stage(ca):
        arrived(recv2.at[ca], 3 + ca)
        work[...] = flat(recv2.at[ca])
        parts = [work[pl.ds(i, n, stride=per), :] for i in range(per)]
        for i in range(per):
            ea, eb, lhs = parts[i], parts[per - 1 - i], tab
            if ca == 0 and i in (0, per - 1):
                eb = jnp.where(at_zero, ea, eb)
            if ca == 0 and i == 0:
                lhs = tab_zero
            ra = pltpu.roll(ea, half, 1)
            rb = pltpu.roll(eb, half, 1)
            z = jnp.concatenate(
                [
                    (ea * m1).astype(BF16),
                    (ra * m2).astype(BF16),
                    (eb * m3 + rb * m4).astype(BF16),
                    (eb * m4 + rb * m5).astype(BF16),
                ],
                axis=0,
            )
            work[pl.ds(i, n, stride=per), :] = dot(lhs, z) * scale
        send3[ca] = blocks(work[...])
        post(send3.at[ca], recv3.at[ca], 6 + ca)

    piece_rows = part // 2
    pending = []

    def ring(ca, slot, h, peer, s_sem, r_sem):
        at = gath.at[ca].at[slot].at[pl.ds(h * piece_rows, piece_rows)]
        return pltpu.make_async_remote_copy(
            src_ref=at,
            dst_ref=at,
            send_sem=s_sem,
            recv_sem=r_sem,
            device_id={"col": peer},
            device_id_type=MESH,
        )

    def go(*args):
        copy = ring(*args)
        copy.start()
        pending.append(copy)

    def gather_start(ca):
        arrived(recv3.at[ca], 6 + ca)
        gath[ca, col] = dot(order, flat(recv3.at[ca]).astype(BF16)).astype(BF16)
        go(ca, col, 0, right, rs_sem.at[ca, 0], rr_sem.at[ca, 0])
        go(ca, col, 1, left, ls_sem.at[ca, 0], lr_sem.at[ca, 0])
        go(ca, col, 1, right, rs_sem.at[ca, 1], rr_sem.at[ca, 1])
        go(ca, col, 0, left, ls_sem.at[ca, 1], lr_sem.at[ca, 1])
        go(ca, col, 0, sib, ss_sem.at[ca, 0], sr_sem.at[ca, 0])
        go(ca, col, 1, sib, ss_sem.at[ca, 1], sr_sem.at[ca, 1])

    steps = ncol // 2 - 1

    def gather_step(ca, i):
        dist = i // 2 + 1
        slot = lax.rem(col + ncol - 2 * dist, ncol)
        h = i % 2
        ring(ca, slot, h, right, rs_sem.at[ca, i], rr_sem.at[ca, i]).wait_recv()
        if i + 2 < steps:
            go(ca, slot, h, right, rs_sem.at[ca, i + 2], rr_sem.at[ca, i + 2])
        go(ca, slot, h, sib, ss_sem.at[ca, 2 + 2 * i], sr_sem.at[ca, 2 + 2 * i])
        slot = lax.rem(col + 2 * dist, ncol)
        h = 1 - i % 2
        ring(ca, slot, h, left, ls_sem.at[ca, i], lr_sem.at[ca, i]).wait_recv()
        if i + 2 < steps:
            go(ca, slot, h, left, ls_sem.at[ca, i + 2], lr_sem.at[ca, i + 2])
        go(ca, slot, h, sib, ss_sem.at[ca, 3 + 2 * i], sr_sem.at[ca, 3 + 2 * i])

    def project(ca):
        for i in range(2 * steps + 2):
            ring(ca, 0, 0, sib, ss_sem.at[ca, i], sr_sem.at[ca, i]).wait_recv()
        acc = None
        for y in range(ncol // 2):
            lhs = jnp.concatenate([gath[ca, 2 * y], gath[ca, 2 * y + 1]], axis=1)
            term = dot(lhs, wout[pl.ds(2 * width * y, 2 * width), :])
            acc = term if acc is None else acc + term
        low = part // 2
        out[pl.ds(low * ca, low), :] = acc[:low].astype(BF16)
        upper[pl.ds(low * (CHUNKS - 1 - ca), low), :] = acc[low:]

    def steps_of(ca, first, last):
        for i in range(first, last):
            gather_step(ca, i)

    outer_stage(0)
    post(send2.at[2], recv2.at[2], 5)
    outer_stage(1)
    gather_start(0)
    steps_of(0, 0, 3)
    outer_stage(2)
    steps_of(0, 3, steps)
    gather_start(1)
    project(0)
    steps_of(1, 0, 4)
    gather_start(2)
    steps_of(1, 4, steps)
    project(1)
    steps_of(2, 0, steps)
    project(2)
    edge = [upper[pl.ds(n * k, 1), :] for k in range(n // 4)]
    for k in range(n // 4):
        upper[pl.ds(n * ((k + 1) % (n // 4)), 1), :] = edge[k]
    out[pl.ds(rows // 2, rows // 2), :] = upper[...].astype(BF16)
    for copy in pending:
        copy.wait_send()
    for which in range(3 * CHUNKS):
        rest = recv1.at[0].at[pl.ds(0, n - 1)]
        pltpu.make_async_copy(rest, rest, xs.at[which]).wait()


def on_device(tokens, proj_in, proj_out):
    n = lax.axis_size("row")
    ncol = lax.axis_size("col")
    rows, depth = tokens.shape
    width = proj_in.shape[1]
    part = rows // CHUNKS
    steps = ncol // 2 - 1
    anywhere = pl.BlockSpec(memory_space=pl.ANY)
    message = pltpu.VMEM((CHUNKS, n, part // n, width), BF16)
    dma = pltpu.SemaphoreType.DMA
    return pl.pallas_call(
        functools.partial(kernel, n, ncol),
        out_shape=jax.ShapeDtypeStruct((rows, proj_out.shape[1]), BF16),
        in_specs=[anywhere] * 3,
        out_specs=pl.BlockSpec(memory_space=pltpu.VMEM),
        scratch_shapes=[
            pltpu.VMEM(tokens.shape, BF16),
            pltpu.VMEM(proj_in.shape, BF16),
            pltpu.VMEM(proj_out.shape, BF16),
            pltpu.VMEM((CHUNKS, 2 * part, rows), BF16),
            pltpu.VMEM((n, rows), F32),
            pltpu.VMEM((n, rows), F32),
            pltpu.VMEM((part, width), F32),
            pltpu.VMEM((CHUNKS, 2 * part, width), F32),
            message,
            message,
            message,
            message,
            message,
            message,
            pltpu.VMEM((CHUNKS, ncol, part, width), BF16),
            pltpu.VMEM((rows // 2, proj_out.shape[1]), F32),
            dma((CHUNKS + 2,)),
            dma((3 * CHUNKS,)),
            dma((3 * CHUNKS,)),
            dma((CHUNKS, steps)),
            dma((CHUNKS, steps)),
            dma((CHUNKS, steps)),
            dma((CHUNKS, steps)),
            dma((CHUNKS, 2 * steps + 2)),
            dma((CHUNKS, 2 * steps + 2)),
        ],
        compiler_params=pltpu.CompilerParams(
            collective_id=0, has_side_effects=True, vmem_limit_bytes=60 * 1024 * 1024
        ),
    )(tokens, proj_in, proj_out)


def solution(mesh):
    return jax.shard_map(
        on_device,
        mesh=mesh,
        in_specs=(P("row", None), P(None, "col"), P(None, "col")),
        out_specs=P("row", "col"),
        check_vma=False,
    )
```

time: 217 us -> 101 us (0.47)
  matrix products: 60.2 us -> 0 us
  waiting for transfers between devices: 57.3 us -> 0 us
  Pallas kernels: 72.9 us -> 99.3 us
  between operations: 13.7 us -> 0.01 us
  local copies, waits for them, and re-layouts: 8.11 us -> 1.92 us
  other arithmetic: 4.23 us -> 0 us
    dot_general x7 -> x0, matrix products: 60.2 us -> none  [the longest x1 25.8 us: on_device(): h = jnp.dot(ts.astype(BF16), data, preferred_element_type=F32)]
    all_gather x1 -> x0, waiting for transfers between devices: 57.3 us -> none  [on_device(): gathered = lax.all_gather(spectrum, 'col', axis=1, tiled=True)]
    pallas_call x3 -> x1, Pallas kernels: 72.9 us -> 99.3 us  [on_device(): pl.pallas_call(functools.partial(kernel, n, ncol), out_shape=jax.ShapeDty...]
  transfers between devices with their start and end apart: 1 -> 0, of which waited for: 1 -> 0; matrix products, arithmetic and copies ran while one was open for 1% -> 0% of each run, Pallas kernels for 0% -> 0%
where the time goes in v2:
time: 101 us
  Pallas kernels  99.3 us (98%)
  local copies, waits for them, and re-layouts  1.92 us (2%)
    pallas_call x1, Pallas kernels, on_device(): pl.pallas_call(functools.partial(kernel, n, ncol), out_shape=jax.ShapeDty...  99.3 us

profile of v2, /device:TPU:1, one launch (start us, length us, event | category | flops | bytes accessed | tf_op | source)
XLA Modules:
  0.0 101.2 jit_solution(4902775383335622721)
XLA Ops:
  0.0 99.3 %shard_map.37 = bf16[1152,256]{1,0:T(8,128)(2,1)} custom-call(bf16[1152,4096]{1,0:T(8,128)(2,1)} %tokens.1, bf16[4096,128]{1,0:T(8,128)(2,1)} %proj_in.1, bf16[2048,256]{1,0:T(8,128)(2,1)} %proj_out.1), custom_call_target="tpu_custom_call" | custom-call | tf_op jit(solution)/shard_map/pallas_call | solution.py:376
  99.3 1.9 %copy.5 = bf16[1152,256]{1,0:T(8,128)(2,1)} copy(bf16[1152,256]{1,0:T(8,128)(2,1)} %shard_map.37) | data formatting | bytes 1179648

commit v3 on v2

v3 whole, which is shorter than its diff:
```python
import functools
import math

import jax
import jax.numpy as jnp
from jax import lax
from jax.experimental import pallas as pl
from jax.experimental.pallas import tpu as pltpu
from jax.sharding import PartitionSpec as P

MESH = pl.DeviceIdType.MESH
BF16 = jnp.bfloat16
F32 = jnp.float32
CHUNKS = 3
SIZES = (8, 8, 8)


def turn(phase, period):
    wraps = jnp.floor(phase * (1.0 / period) + 0.5)
    x = (phase - wraps * period) * (math.pi / period)
    y = x * x
    s = 1.0 + y * (-1 / 6 + y * (1 / 120 + y * (-1 / 5040 + y * (1 / 362880 + y * (-1 / 39916800)))))
    c = 1.0 + y * (
        -1 / 2 + y * (1 / 24 + y * (-1 / 720 + y * (1 / 40320 + y * (-1 / 3628800 + y * (1 / 479001600)))))
    )
    s = s * x
    return 1.0 - 2.0 * s * s, 2.0 * s * c


def iota(shape, axis):
    return lax.broadcasted_iota(jnp.int32, shape, axis)


def dot(a, b):
    return jnp.dot(a, b, preferred_element_type=F32)


def kernel(
    n,
    ncol,
    tokens,
    proj_in,
    proj_out,
    out,
    tok,
    win,
    wout,
    table,
    base_c,
    base_s,
    work,
    gacc,
    send1,
    recv1,
    upper,
    load_sem,
    xs,
    xr,
    rr_sem,
    lr_sem,
    ss_sem,
    sr_sem,
    *rest,
):
    parts_ = len(SIZES)
    send2, recv2, send3, recv3, gath = (rest[k * parts_ : (k + 1) * parts_] for k in range(5))
    starts = [sum(SIZES[:c]) for c in range(parts_)]
    rank = lax.axis_index("row")
    col = lax.axis_index("col")
    core = lax.rem(col, 2)
    right = lax.rem(col + 2, ncol)
    left = lax.rem(col + ncol - 2, ncol)
    sib = col + 1 - 2 * core
    rows, depth = tokens.shape
    width = proj_in.shape[1]
    half = width // 2
    total = rows * n
    part = rows // CHUNKS
    per = part // n

    barrier = pltpu.get_barrier_semaphore()

    def greet(s, carry):
        pl.semaphore_signal(
            barrier, inc=1, device_id={"row": lax.rem(rank + s, n)}, device_id_type=MESH
        )
        return carry

    lax.fori_loop(1, n, greet, 0)
    for peer in (right, left, sib):
        pl.semaphore_signal(barrier, inc=1, device_id={"col": peer}, device_id_type=MESH)

    load_in = pltpu.make_async_copy(proj_in, win, load_sem.at[CHUNKS])
    load_in.start()
    loads = []
    for c in range(CHUNKS):
        block = pl.ds(c * part, part)
        load = pltpu.make_async_copy(tokens.at[block], tok.at[block], load_sem.at[c])
        load.start()
        loads.append(load)
    load_out = pltpu.make_async_copy(proj_out, wout, load_sem.at[CHUNKS + 1])
    load_out.start()

    def post(src, dst, which):
        def send(peer):
            pltpu.make_async_remote_copy(
                src_ref=src.at[peer],
                dst_ref=dst.at[rank],
                send_sem=xs.at[which],
                recv_sem=xr.at[which],
                device_id={"row": peer},
                device_id_type=MESH,
            ).start()

        def both(s, carry):
            up = rank + (n // 2 - s)
            down = rank - (n // 2 - s)
            send(jnp.where(up >= n, up - n, up))
            send(jnp.where(down < 0, down + n, down))
            return carry

        opposite = rank + n // 2
        send(jnp.where(opposite >= n, opposite - n, opposite))
        lax.fori_loop(1, n // 2, both, 0)
        dst[rank] = src[rank]

    def post2(k):
        post(send2[k], recv2[k], CHUNKS + k)

    def arrived(dst, which):
        rest = dst.at[pl.ds(0, n - 1)]
        pltpu.make_async_copy(rest, rest, xr.at[which]).wait()

    def flat(ref):
        return ref[...].astype(F32).reshape(n * ref.shape[1], width)

    def blocks(value):
        return value.reshape(n, value.shape[0] // n, width).astype(BF16)

    lane = iota((width, width), 1)
    j = iota((width, width), 0)
    l = jnp.where(lane < half, lane, jnp.where(lane == half, half, lane - half))
    cc, sc = turn((j * l).astype(F32), width)
    chan = jnp.where(lane <= half, cc, -sc).astype(BF16)

    load_in.wait()
    for c in range(CHUNKS):
        with jax.named_scope(f"tokens{c}"):
            loads[c].wait()
        with jax.named_scope(f"branch{c}"):
            x = dot(tok[pl.ds(c * part, part), :], win[...]).astype(BF16)
            work[...] = dot(x, chan)
            for p in range(n):
                send1[c, p] = work[pl.ds(p, per, stride=n), :].astype(BF16)
        if c == 0:
            with jax.named_scope("barrier"):
                pl.semaphore_wait(barrier, n - 1 + 3)
        with jax.named_scope(f"post1_{c}"):
            post(send1.at[c], recv1.at[c], c)

    with jax.named_scope("tables"):
        lanes = rows
        li = iota((8, lanes), 1)
        cq = jnp.where(li >= 2 * part, 2, jnp.where(li >= part, 1, 0))
        rem = li - cq * part
        t = n // 2 * (rem // per) + per * cq + rem % per
        time = (n * t + rank).astype(F32)
        ri = iota((8, lanes), 0)
        for g in range(n // 8):
            bc, bs = turn((ri + 8 * g).astype(F32) * time, total)
            base_c[pl.ds(8 * g, 8), :] = bc
            base_s[pl.ds(8 * g, 8), :] = bs

        for c, size in enumerate(SIZES):
            start = starts[c] // 2
            place = ri % size
            lower = place < size // 2
            num = jnp.where(lower, start + place, 25 - start - size + place)
            sigma = jnp.where(lower, 1.0, -1.0).astype(F32)
            wc, ws = turn(num.astype(F32) * time, rows)
            wcs, wss = wc * sigma, ws * sigma
            each = 8 // size
            row = 2 * n * starts[c]

            def unit(u, wc=wc, ws=ws, wcs=wcs, wss=wss, each=each):
                bc = base_c[pl.ds(u * each, 1), :]
                bs = base_s[pl.ds(u * each, 1), :]
                if each == 2:
                    bc = jnp.where(ri < 4, bc, base_c[pl.ds(2 * u + 1, 1), :])
                    bs = jnp.where(ri < 4, bs, base_s[pl.ds(2 * u + 1, 1), :])
                return wc * bc - wss * bs, ws * bc + wcs * bs

            def put(pair, first, second, row=row, size=size):
                at = pl.multiple_of(row + 16 * pair, 16)
                table[pl.ds(at, 16), :] = jnp.concatenate([first[0], second[0]], axis=0).astype(BF16)
                at = pl.multiple_of(row + n * size + 16 * pair, 16)
                table[pl.ds(at, 16), :] = jnp.concatenate([first[1], second[1]], axis=0).astype(BF16)

            def body(pair, carry, unit=unit, put=put):
                put(pair, unit(2 * pair), unit(2 * pair + 1))
                return carry

            lax.fori_loop(0, n * size // 16, body, 0)
            if c == 0:
                mc, ms = turn(jnp.float32(12.0) * time, rows)
                oc, os = unit(0)
                mid = ri == size - 1
                put(0, (jnp.where(mid, mc, oc), jnp.where(mid, ms, os)), unit(1))

    with jax.named_scope("tables2"):
        bi = iota((n, 4 * n), 0)
        pi = iota((n, 4 * n), 1)
        quarter = jnp.where(pi >= 3 * n, 3, jnp.where(pi >= 2 * n, 2, jnp.where(pi >= n, 1, 0)))
        pp = pi - quarter * n

        def outer(flip):
            bb = jnp.where(quarter < 2, bi, flip - bi)
            oc, os = turn((bb * pp).astype(F32), n)
            return jnp.where((quarter == 0) | (quarter == 2), oc, os)

        at_zero = rank == 0
        tab = outer(n - 1)
        tab_zero = jnp.where(at_zero, outer(n), tab).astype(BF16)
        tab = tab.astype(BF16)

        qr = iota((width, width), 0)
        qc = iota((width, width), 1)
        chosen = jnp.where(qr <= half, qr, width + half - qr)
        swap = jnp.where(qc == chosen, 1.0, 0.0).astype(BF16)
        load_out.wait()

        def reorder(g, carry):
            at = pl.ds(pl.multiple_of(g * width, width), width)
            wout[at, :] = dot(swap, wout[at, :]).astype(BF16)
            return carry

        lax.fori_loop(0, ncol, reorder, 0)

        orders = {}
        for size in sorted(set(SIZES)):
            pr = iota((n * size, n * size), 0)
            pc = iota((n * size, n * size), 1)
            want_i = pr // n
            want_e = pr - want_i * n
            want_d = jnp.where(want_i < size // 2, want_e, jnp.where(want_e == 0, 0, n - want_e))
            orders[size] = jnp.where(pc == want_d * size + want_i, 1.0, 0.0).astype(BF16)

    sign = jnp.where(iota((part, width), 1) < half, 1.0, -1.0).astype(F32)
    for c in range(CHUNKS):
        with jax.named_scope(f"wait1_{c}"):
            arrived(recv1.at[c], c)
        data = flat(recv1.at[c]).astype(BF16)
        for k, size in enumerate(SIZES):
            at = pl.ds(2 * n * starts[k], 2 * n * size)
            got = dot(table[at, pl.ds(c * part, part)], data)
            if c > 0:
                got = gacc[at, :] + got
            if c < CHUNKS - 1:
                gacc[at, :] = got
            else:
                value = got[: n * size] + pltpu.roll(got[n * size :], half, 1) * sign[: n * size]
                send2[k][...] = blocks(value)
                if k < 2:
                    with jax.named_scope(f"post2_{k}"):
                        post2(k)

    lane48 = iota((n, width), 1)
    m1 = jnp.where((lane48 == 0) | (lane48 == half), 0.5, jnp.where(lane48 < half, 1.0, 0.0)).astype(F32)
    m2 = jnp.where(lane48 == half, -0.5, m1).astype(F32)
    m3 = jnp.where((lane48 == 0) | (lane48 == half), 0.5, 0.0).astype(F32)
    m4 = jnp.where(lane48 > half, 1.0, 0.0).astype(F32)
    m5 = jnp.where(lane48 == half, -0.5, m3).astype(F32)
    scale = 1.0 / math.sqrt(total * width)

    def outer_wait(k):
        arrived(recv2[k], CHUNKS + k)

    def outer_stage(k):
        size = SIZES[k]
        held = work.at[pl.ds(0, n * size)]
        held[...] = flat(recv2[k])
        parts = [held[pl.ds(i, n, stride=size), :] for i in range(size)]
        for i in range(size):
            ea, eb, lhs = parts[i], parts[size - 1 - i], tab
            if k == 0 and i in (0, size - 1):
                eb = jnp.where(at_zero, ea, eb)
            if k == 0 and i == 0:
                lhs = tab_zero
            ra = pltpu.roll(ea, half, 1)
            rb = pltpu.roll(eb, half, 1)
            z = jnp.concatenate(
                [
                    (ea * m1).astype(BF16),
                    (ra * m2).astype(BF16),
                    (eb * m3 + rb * m4).astype(BF16),
                    (eb * m4 + rb * m5).astype(BF16),
                ],
                axis=0,
            )
            held[pl.ds(i, n, stride=size), :] = dot(lhs, z) * scale
        send3[k][...] = blocks(held[...])
        post(send3[k], recv3[k], CHUNKS + parts_ + k)


    def ring(ca, slot, h, peer, s_sem, r_sem):
        piece_rows = n * SIZES[ca] // 2
        at = gath[ca].at[slot].at[pl.ds(h * piece_rows, piece_rows)]
        return pltpu.make_async_remote_copy(
            src_ref=at,
            dst_ref=at,
            send_sem=s_sem,
            recv_sem=r_sem,
            device_id={"col": peer},
            device_id_type=MESH,
        )

    def go(*args):
        ring(*args).start()

    def gather_start(ca):
        with jax.named_scope(f"wait3_{ca}"):
            arrived(recv3[ca], CHUNKS + parts_ + ca)
        gath[ca][col] = dot(orders[SIZES[ca]], flat(recv3[ca]).astype(BF16)).astype(BF16)
        go(ca, col, 0, right, ss_sem.at[ca], rr_sem.at[ca, 0])
        go(ca, col, 1, left, ss_sem.at[ca], lr_sem.at[ca, 0])
        go(ca, col, 1, right, ss_sem.at[ca], rr_sem.at[ca, 1])
        go(ca, col, 0, left, ss_sem.at[ca], lr_sem.at[ca, 1])
        go(ca, col, 0, sib, ss_sem.at[ca], sr_sem.at[ca])
        go(ca, col, 1, sib, ss_sem.at[ca], sr_sem.at[ca])

    steps = ncol // 2 - 1

    def gather_step(ca, i):
        dist = i // 2 + 1
        slot = lax.rem(col + ncol - 2 * dist, ncol)
        h = i % 2
        ring(ca, slot, h, right, ss_sem.at[ca], rr_sem.at[ca, i]).wait_recv()
        if i + 2 < steps:
            go(ca, slot, h, right, ss_sem.at[ca], rr_sem.at[ca, i + 2])
        go(ca, slot, h, sib, ss_sem.at[ca], sr_sem.at[ca])
        slot = lax.rem(col + 2 * dist, ncol)
        h = 1 - i % 2
        ring(ca, slot, h, left, ss_sem.at[ca], lr_sem.at[ca, i]).wait_recv()
        if i + 2 < steps:
            go(ca, slot, h, left, ss_sem.at[ca], lr_sem.at[ca, i + 2])
        go(ca, slot, h, sib, ss_sem.at[ca], sr_sem.at[ca])

    def project(ca):
        whole = gath[ca].at[pl.ds(0, ncol // 2)]
        pltpu.make_async_copy(whole, whole, sr_sem.at[ca]).wait()
        acc = None
        for y in range(ncol // 2):
            lhs = jnp.concatenate([gath[ca][2 * y], gath[ca][2 * y + 1]], axis=1)
            term = dot(lhs, wout[pl.ds(2 * width * y, 2 * width), :])
            acc = term if acc is None else acc + term
        low = n * SIZES[ca] // 2
        first = n * starts[ca] // 2
        out[pl.ds(first, low), :] = acc[:low].astype(BF16)
        upper[pl.ds(rows // 2 - first - low, low), :] = acc[low:]

    def steps_of(ca, first, last):
        for i in range(first, last):
            gather_step(ca, i)

    sent = [recv1.at[0]] * CHUNKS + list(recv2) + list(recv3)

    def drain(ca):
        whole = gath[ca].at[pl.ds(0, 2 * steps + 1)]
        pltpu.make_async_copy(whole, whole, ss_sem.at[ca]).wait()

    def drain_exchanges():
        for which, ref in enumerate(sent):
            whole = ref.at[pl.ds(0, n - 1)]
            pltpu.make_async_copy(whole, whole, xs.at[which]).wait()

    with jax.named_scope("W0"):
        outer_wait(0)
    with jax.named_scope("O0"):
        outer_stage(0)
    with jax.named_scope("P2"):
        post2(2)
    with jax.named_scope("W1"):
        outer_wait(1)
    with jax.named_scope("O1"):
        outer_stage(1)
    with jax.named_scope("G0"):
        gather_start(0)
    with jax.named_scope("W2"):
        outer_wait(2)
    with jax.named_scope("O2"):
        outer_stage(2)
    with jax.named_scope("S00"):
        gather_step(0, 0)
    with jax.named_scope("S01"):
        gather_step(0, 1)
    with jax.named_scope("G1"):
        gather_start(1)
    with jax.named_scope("S02"):
        gather_step(0, 2)
    with jax.named_scope("S03"):
        gather_step(0, 3)
    with jax.named_scope("S10"):
        gather_step(1, 0)
    with jax.named_scope("S11"):
        gather_step(1, 1)
    with jax.named_scope("S04"):
        gather_step(0, 4)
    with jax.named_scope("S05"):
        gather_step(0, 5)
    with jax.named_scope("G2"):
        gather_start(2)
    with jax.named_scope("S12"):
        gather_step(1, 2)
    with jax.named_scope("S13"):
        gather_step(1, 3)
    with jax.named_scope("S06"):
        gather_step(0, 6)
    with jax.named_scope("S20"):
        gather_step(2, 0)
    with jax.named_scope("S21"):
        gather_step(2, 1)
    with jax.named_scope("S14"):
        gather_step(1, 4)
    with jax.named_scope("S15"):
        gather_step(1, 5)
    with jax.named_scope("S22"):
        gather_step(2, 2)
    with jax.named_scope("S23"):
        gather_step(2, 3)
    with jax.named_scope("S16"):
        gather_step(1, 6)
    with jax.named_scope("J0"):
        project(0)
    with jax.named_scope("S24"):
        gather_step(2, 4)
    with jax.named_scope("S25"):
        gather_step(2, 5)
    with jax.named_scope("D"):
        for ca in range(parts_ - 1):
            drain(ca)
        drain_exchanges()
    with jax.named_scope("S26"):
        gather_step(2, 6)
    with jax.named_scope("J1"):
        project(1)
    with jax.named_scope("J2"):
        project(2)
    with jax.named_scope("finish"):
        edge = [upper[pl.ds(n * k, 1), :] for k in range(n // 4)]
        for k in range(n // 4):
            upper[pl.ds(n * ((k + 1) % (n // 4)), 1), :] = edge[k]
        out[pl.ds(rows // 2, rows // 2), :] = upper[...].astype(BF16)
    drain(parts_ - 1)


def on_device(tokens, proj_in, proj_out):
    n = lax.axis_size("row")
    ncol = lax.axis_size("col")
    rows, depth = tokens.shape
    width = proj_in.shape[1]
    part = rows // CHUNKS
    steps = ncol // 2 - 1
    count = len(SIZES)
    anywhere = pl.BlockSpec(memory_space=pltpu.HBM)
    message = pltpu.VMEM((CHUNKS, n, part // n, width), BF16)
    dma = pltpu.SemaphoreType.DMA
    return pl.pallas_call(
        functools.partial(kernel, n, ncol),
        out_shape=pltpu.VMEM((rows, proj_out.shape[1]), BF16),
        in_specs=[anywhere] * 3,
        out_specs=pl.BlockSpec(memory_space=pltpu.VMEM),
        scratch_shapes=[
            pltpu.VMEM(tokens.shape, BF16),
            pltpu.VMEM(proj_in.shape, BF16),
            pltpu.VMEM(proj_out.shape, BF16),
            pltpu.VMEM((2 * rows, rows), BF16),
            pltpu.VMEM((n, rows), F32),
            pltpu.VMEM((n, rows), F32),
            pltpu.VMEM((part, width), F32),
            pltpu.VMEM((2 * rows, width), F32),
            message,
            message,
            pltpu.VMEM((rows // 2, proj_out.shape[1]), F32),
            dma((CHUNKS + 2,)),
            dma((CHUNKS + 2 * count,)),
            dma((CHUNKS + 2 * count,)),
            dma((count, steps)),
            dma((count, steps)),
            dma((count,)),
            dma((count,)),
            *(pltpu.VMEM((n, size, width), BF16) for _ in range(4) for size in SIZES),
            *(pltpu.VMEM((ncol, n * size, width), BF16) for size in SIZES),
        ],
        compiler_params=pltpu.CompilerParams(
            collective_id=0, has_side_effects=True, vmem_limit_bytes=66000000
        ),
    )(tokens, proj_in, proj_out)


def solution(mesh):
    return jax.shard_map(
        on_device,
        mesh=mesh,
        in_specs=(P("row", None), P(None, "col"), P(None, "col")),
        out_specs=P("row", "col"),
        check_vma=False,
    )
```

time: 101 us -> 83.3 us (0.82)
  Pallas kernels: 99.3 us -> 82.4 us
  local copies, waits for them, and re-layouts: 1.92 us -> 0.82 us
    pallas_call x1, Pallas kernels: 99.3 us -> 82.4 us  [on_device(): pl.pallas_call(functools.partial(kernel, n, ncol), out_shape=pltpu.VMEM((...]
    unnamed x1, local copies, waits for them, and re-layouts: 1.92 us -> 0.82 us
where the time goes in v3:
time: 83.3 us; the launch traced here: 83.2 us
  Pallas kernels  82.4 us (99%)
    pallas_call x1, Pallas kernels, on_device(): pl.pallas_call(functools.partial(kernel, n, ncol), out_shape=pltpu.VMEM((...  82.4 us

profile of v3, /device:TPU:1, one launch (start us, length us, event | category | flops | bytes accessed | tf_op | source)
XLA Modules:
  0.0 83.2 jit_solution(11496729037317232067)
XLA Ops:
  0.0 82.4 %shard_map.37 = bf16[1152,256]{1,0:T(8,128)(2,1)S(1)} custom-call(bf16[1152,4096]{1,0:T(8,128)(2,1)} %tokens.1, bf16[4096,128]{1,0:T(8,128)(2,1)} %proj_in.1, bf16[2048,256]{1,0:T(8,128)(2,1)} %proj_out.1), custom_call_target="tpu_custom_call" | custom-call | tf_op jit(solution)/shard_map/pallas_call | solution.py:467
  82.4 0.8 copy.5

commit v4 on v3

--- a/solution.py
+++ b/solution.py
@@ -325,8 +325,8 @@
         go(ca, col, 1, left, ss_sem.at[ca], lr_sem.at[ca, 0])
         go(ca, col, 1, right, ss_sem.at[ca], rr_sem.at[ca, 1])
         go(ca, col, 0, left, ss_sem.at[ca], lr_sem.at[ca, 1])
-        go(ca, col, 0, sib, ss_sem.at[ca], sr_sem.at[ca])
-        go(ca, col, 1, sib, ss_sem.at[ca], sr_sem.at[ca])
+        go(ca, col, 0, sib, ss_sem.at[ca], sr_sem.at[ca, 0])
+        go(ca, col, 1, sib, ss_sem.at[ca], sr_sem.at[ca, 0])
 
     steps = ncol // 2 - 1
 
@@ -337,21 +337,27 @@
         ring(ca, slot, h, right, ss_sem.at[ca], rr_sem.at[ca, i]).wait_recv()
         if i + 2 < steps:
             go(ca, slot, h, right, ss_sem.at[ca], rr_sem.at[ca, i + 2])
-        go(ca, slot, h, sib, ss_sem.at[ca], sr_sem.at[ca])
+        go(ca, slot, h, sib, ss_sem.at[ca], sr_sem.at[ca, i // (steps - 1)])
         slot = lax.rem(col + 2 * dist, ncol)
         h = 1 - i % 2
         ring(ca, slot, h, left, ss_sem.at[ca], lr_sem.at[ca, i]).wait_recv()
         if i + 2 < steps:
             go(ca, slot, h, left, ss_sem.at[ca], lr_sem.at[ca, i + 2])
-        go(ca, slot, h, sib, ss_sem.at[ca], sr_sem.at[ca])
+        go(ca, slot, h, sib, ss_sem.at[ca], sr_sem.at[ca, i // (steps - 1)])
 
     def project(ca):
-        whole = gath[ca].at[pl.ds(0, ncol // 2)]
-        pltpu.make_async_copy(whole, whole, sr_sem.at[ca]).wait()
         acc = None
-        for y in range(ncol // 2):
+        for k in range(ncol // 2):
+            if k == 0:
+                whole = gath[ca].at[pl.ds(0, ncol // 2 - 1)]
+                pltpu.make_async_copy(whole, whole, sr_sem.at[ca, 0]).wait()
+            if k == ncol // 2 - 1:
+                whole = gath[ca].at[pl.ds(0, 1)]
+                pltpu.make_async_copy(whole, whole, sr_sem.at[ca, 1]).wait()
+            y = lax.rem(col // 2 + (ncol // 4 + 1) + k, ncol // 2)
             lhs = jnp.concatenate([gath[ca][2 * y], gath[ca][2 * y + 1]], axis=1)
-            term = dot(lhs, wout[pl.ds(2 * width * y, 2 * width), :])
+            at = pl.ds(pl.multiple_of(2 * width * y, 2 * width), 2 * width)
+            term = dot(lhs, wout[at, :])
             acc = term if acc is None else acc + term
         low = n * SIZES[ca] // 2
         first = n * starts[ca] // 2
@@ -487,7 +493,7 @@
             dma((count, steps)),
             dma((count, steps)),
             dma((count,)),
-            dma((count,)),
+            dma((count, 2)),
             *(pltpu.VMEM((n, size, width), BF16) for _ in range(4) for size in SIZES),
             *(pltpu.VMEM((ncol, n * size, width), BF16) for size in SIZES),
         ],

time: 83.3 us -> 82.7 us (level)
  no operation moved by 1% of the time
where the time goes in v4:
time: 82.7 us; the launch traced here: 82.6 us
  Pallas kernels  81.7 us (99%)
    pallas_call x1, Pallas kernels, on_device(): pl.pallas_call(functools.partial(kernel, n, ncol), out_shape=pltpu.VMEM((...  81.7 us

profile of v4, /device:TPU:1, one launch (start us, length us, event | category | flops | bytes accessed | tf_op | source)
XLA Modules:
  0.0 82.6 jit_solution(17182291317618330942)
XLA Ops:
  0.0 81.7 %shard_map.37 = bf16[1152,256]{1,0:T(8,128)(2,1)S(1)} custom-call(bf16[1152,4096]{1,0:T(8,128)(2,1)} %tokens.1, bf16[4096,128]{1,0:T(8,128)(2,1)} %proj_in.1, bf16[2048,256]{1,0:T(8,128)(2,1)} %proj_out.1), custom_call_target="tpu_custom_call" | custom-call | tf_op jit(solution)/shard_map/pallas_call | solution.py:473
  81.8 0.8 copy.5
